TPU v7x, 32 devices: a whole 2x2x4 slice. The times are simulated.
32 devices in a mesh: sp: 16 (over z, y, x), tp: 2 (over core).
Axes of the slice: x: 2, y: 2, z: 4, core: 2. Of those that a mesh axis runs over, the one named last changes fastest.
Arguments:
- residual: bfloat16 [4096, 2048], P(('sp', 'tp')), as said below
- outer_gate: bfloat16 [4096, 1024], P('sp', 'tp'), may hold values from -6 to 6
- conv_input: bfloat16 [4096, 1024], P('sp', 'tp'), as said below
- conv_value: bfloat16 [4096, 1024], P('sp', 'tp'), may hold values from -6 to 6
- doc_ids: int32 [4096], P('sp'), may hold values from 0 to 7, never falling along the last dimension, each value on 1 to 1024 neighbouring positions
- conv_taps: bfloat16 [3, 1024], P(None, 'tp'), may hold values from -3.5 to 3.5
- branch_gain: bfloat16 [1024], P('tp'), may hold values from 0.099609375 to 1.8984375
- out_weight: bfloat16 [1024, 2048], replicated, may hold values from -0.1875 to 0.1875
- ffn_gain: bfloat16 [2048], replicated, may hold values from 0.099609375 to 1.8984375
- route_ids: int32 [4096, 4], P(('sp', 'tp')), may hold values from 0 to 31, all different within a row; in each aligned block of 128 rows (0 to 127, 128 to 255, ...) at most 32 rows name the same one
- route_weight: float32 [4096, 4], P(('sp', 'tp')), may hold values from 0.2 to 1
- shared_gate: bfloat16 [2048, 512], replicated, may hold values from -0.125 to 0.125
- shared_up: bfloat16 [2048, 512], replicated, may hold values from -0.125 to 0.125
- shared_down: bfloat16 [512, 2048], replicated, may hold values from -0.25 to 0.25
- expert_gate: bfloat16 [32, 2048, 512], P(('sp', 'tp')), may hold values from -0.125 to 0.125
- expert_up: bfloat16 [32, 2048, 512], P(('sp', 'tp')), may hold values from -0.125 to 0.125
- expert_down: bfloat16 [32, 512, 2048], P(('sp', 'tp')), may hold values from -0.25 to 0.25
Outputs:
- layer_out: bfloat16 [4096, 2048], P(('sp', 'tp'))
Inputs may be any that keep to these rules, and one draw needn't show every extreme that they name: `route_ids`: each row names 4 different experts. Within each aligned block of 128 rows (the rows of one device) no expert is named by more than 32 rows, and in every draw some expert is named by exactly 32 rows of some block. `doc_ids`: document numbers start at 0 and never fall along the sequence; each document has 1 to 1024 positions. `residual`: Real-valued, of order one. `conv_input`: Real-valued, of order one.
All inputs are finite; a program needn't handle non-finite values.
Results may differ from a plain program's by a relative error of at most 0.012.
Values may be sent and summed in bfloat16 or wider, within the bound.
A program may use at most 128 MiB of HBM per device.

v0:
```python
import jax
import jax.numpy as jnp
from jax import lax
from jax.sharding import PartitionSpec as P

norm_eps = 1e-06


def from_behind(value, axis, by):
    peers = lax.axis_size(axis)
    pairs = [(i, i + by) for i in range(peers) if 0 <= i + by < peers]
    return lax.ppermute(value, axis, pairs)


def expert_apply(arrived, gate_w, up_w, down_w):
    flat_rows = arrived.reshape(-1, arrived.shape[-1])
    hidden = (
        jax.nn.silu(jnp.dot(flat_rows, gate_w, preferred_element_type=jnp.float32))
        * jnp.dot(flat_rows, up_w, preferred_element_type=jnp.float32)
    ).astype(jnp.bfloat16)
    result = jnp.dot(hidden, down_w, preferred_element_type=jnp.float32).astype(jnp.bfloat16)
    return result.reshape(arrived.shape)


def shards(
    residual,
    outer_gate,
    conv_input,
    conv_value,
    doc_ids,
    conv_taps,
    branch_gain,
    out_weight,
    ffn_gain,
    route_ids,
    route_weight,
    shared_gate,
    shared_up,
    shared_down,
    expert_gate,
    expert_up,
    expert_down,
):
    seq_rows = conv_input.shape[0]
    half_width = conv_input.shape[1]
    tap_count = conv_taps.shape[0]
    lead_rows = tap_count - 1
    doc_float = doc_ids.astype(jnp.float32)
    prev_input, prev_value, prev_doc = from_behind(
        (
            conv_input[seq_rows - lead_rows :],
            conv_value[seq_rows - lead_rows :],
            doc_float[seq_rows - lead_rows :].astype(jnp.bfloat16),
        ),
        "sp",
        1,
    )
    source = jnp.concatenate(
        [
            prev_input.astype(jnp.float32) * prev_value.astype(jnp.float32),
            conv_input.astype(jnp.float32) * conv_value.astype(jnp.float32),
        ],
        axis=0,
    )
    doc_extended = jnp.concatenate([prev_doc.astype(jnp.float32), doc_float], axis=0)
    mixed_conv = jnp.zeros((seq_rows, half_width), jnp.float32)
    for tap in range(tap_count):
        same_doc = (doc_extended[tap : tap + seq_rows] == doc_float).astype(jnp.float32)[:, None]
        mixed_conv = (
            mixed_conv
            + conv_taps[tap].astype(jnp.float32)[None, :] * source[tap : tap + seq_rows] * same_doc
        )
    branch = outer_gate.astype(jnp.float32) * mixed_conv
    square_total = lax.psum(jnp.sum(branch * branch, axis=1, keepdims=True), "tp")
    inv_rms = lax.rsqrt(square_total / (half_width * lax.axis_size("tp")) + norm_eps)
    normed = (branch * inv_rms * branch_gain.astype(jnp.float32)[None, :]).astype(jnp.bfloat16)
    local_rows = residual.shape[0]
    token_rows = lax.all_to_all(normed, "tp", split_axis=0, concat_axis=1, tiled=True)
    update = jnp.dot(token_rows, out_weight, preferred_element_type=jnp.float32)
    middle = (residual.astype(jnp.float32) + update).astype(jnp.bfloat16)
    mid_float = middle.astype(jnp.float32)
    mid_rms = lax.rsqrt(jnp.mean(mid_float * mid_float, axis=1, keepdims=True) + norm_eps)
    ffn_in = (mid_float * mid_rms * ffn_gain.astype(jnp.float32)[None, :]).astype(jnp.bfloat16)
    shared_hidden = (
        jax.nn.silu(jnp.dot(ffn_in, shared_gate, preferred_element_type=jnp.float32))
        * jnp.dot(ffn_in, shared_up, preferred_element_type=jnp.float32)
    ).astype(jnp.bfloat16)
    shared_out = jnp.dot(shared_hidden, shared_down, preferred_element_type=jnp.float32)
    model_width = residual.shape[1]
    top_count = route_ids.shape[1]
    seq_devices = lax.axis_size("sp")
    core_devices = lax.axis_size("tp")
    expert_count = seq_devices * core_devices
    capacity = local_rows * core_devices * top_count // expert_count
    flat_expert = route_ids.reshape(-1)
    onehot = (flat_expert[:, None] == jnp.arange(expert_count, dtype=jnp.int32)[None, :]).astype(
        jnp.int32
    )
    slot_rank = jnp.sum(onehot * (jnp.cumsum(onehot, axis=0) - onehot), axis=1)
    slot_of = flat_expert * capacity + slot_rank
    token_index = jnp.arange(local_rows * top_count, dtype=jnp.int32) // top_count
    slot_source = (
        jnp.full((expert_count * capacity,), local_rows, jnp.int32).at[slot_of].set(token_index)
    )
    padded_in = jnp.concatenate([ffn_in, jnp.zeros((1, model_width), jnp.bfloat16)], axis=0)
    outgoing = padded_in[slot_source].reshape(expert_count, capacity, model_width)
    gate_w = expert_gate[0]
    up_w = expert_up[0]
    down_w = expert_down[0]
    result = expert_apply(
        lax.all_to_all(outgoing, ("sp", "tp"), split_axis=0, concat_axis=0, tiled=True),
        gate_w,
        up_w,
        down_w,
    )
    returned = lax.all_to_all(result, ("sp", "tp"), split_axis=0, concat_axis=0, tiled=True)
    returned_rows = returned.reshape(expert_count * capacity, model_width)[slot_of]
    weighted = (
        returned_rows.astype(jnp.float32).reshape(local_rows, top_count, model_width)
        * route_weight[:, :, None]
    )
    routed = jnp.sum(weighted, axis=1)
    return (mid_float + shared_out + routed).astype(jnp.bfloat16)


def solution(mesh):
    placed = (
        P(("sp", "tp"), None),
        P("sp", "tp"),
        P("sp", "tp"),
        P("sp", "tp"),
        P("sp"),
        P(None, "tp"),
        P("tp"),
        P(),
        P(),
        P(("sp", "tp"), None),
        P(("sp", "tp"), None),
        P(),
        P(),
        P(),
        P(("sp", "tp"), None, None),
        P(("sp", "tp"), None, None),
        P(("sp", "tp"), None, None),
    )
    return jax.shard_map(
        shards, mesh=mesh, in_specs=placed, out_specs=P(("sp", "tp"), None), check_vma=False
    )
```

profile of v0, /device:TPU:25, one launch (start us, length us, event | category | flops | bytes accessed | tf_op | source)
XLA Modules:
  0.0 275.1 jit_solution(576771368202937796)
XLA Ops:
  0.0 0.8 convert_convert_fusion
  0.9 3.1 %collective-permute-start.2 = (bf16[2]{0:T(256)(128)(2,1)S(1)}, bf16[2]{0:T(256)(128)(2,1)S(1)}, u32[]{:S(2)}, u32[]{:S(2)}) collective-permute-start(bf16[2]{0:T(256)(128)(2,1)S(1)} %slice.41), channel_id=1, source_target_pairs={{0,2},{2,4},{4,6},{6,8},{8,10},{10,12},{12,14},{14,16},{16,18},{18... | collective-permute-start | bytes 20 | tf_op jit(solution)/shard_map/ppermute | solution.py:12
  4.7 3.1 %collective-permute-start = (bf16[2,512]{1,0:T(2,128)(2,1)S(1)}, bf16[2,512]{1,0:T(2,128)(2,1)S(1)}, u32[]{:S(2)}, u32[]{:S(2)}) collective-permute-start(bf16[2,512]{1,0:T(2,128)(2,1)S(1)} %slice.38), channel_id=1, source_target_pairs={{0,2},{2,4},{4,6},{6,8},{8,10},{10,12},{12,14},{14,16},{16,18},{18... | collective-permute-start | bytes 6152 | tf_op jit(solution)/shard_map/ppermute | solution.py:12
  8.6 3.1 %collective-permute-start.1 = (bf16[2,512]{1,0:T(2,128)(2,1)S(1)}, bf16[2,512]{1,0:T(2,128)(2,1)S(1)}, u32[]{:S(2)}, u32[]{:S(2)}) collective-permute-start(bf16[2,512]{1,0:T(2,128)(2,1)S(1)} %slice.39), channel_id=1, source_target_pairs={{0,2},{2,4},{4,6},{6,8},{8,10},{10,12},{12,14},{14,16},{16,18},{18... | collective-permute-start | bytes 6152 | tf_op jit(solution)/shard_map/ppermute | solution.py:12
  11.7 1.1 convert_multiply_fusion
  16.7 1.2 reduce-window.6
  18.4 2.4 scatter_custom_fusion
  21.8 1.3 multiply_reduce_fusion.2
  23.1 3.6 %psum.7 = f32[256,1]{0,1:T(1,128)S(1)} all-reduce(f32[256,1]{0,1:T(1,128)S(1)} %bitcast.69), channel_id=1, replica_groups=mesh['sp'=16,'tp'=2] {'tp'}, use_global_device_ids=true, to_apply=%region_1.0 | all-reduce | flops 256 | bytes 2048 | tf_op jit(solution)/shard_map/psum | solution.py:74
  26.9 3.9 %all_to_all.29 = bf16[2,128,512]{2,1,0:T(8,128)(2,1)S(1)} all-to-all(bf16[2,128,512]{2,1,0:T(8,128)(2,1)S(1)} %bitcast.60), channel_id=1, replica_groups=mesh['sp'=16,'tp'=2] {'tp'}, dimensions={0} | all-to-all | bytes 524288 | tf_op jit(solution)/shard_map/all_to_all | solution.py:78
  31.0 3.1 %multiply_reduce_fusion.1 = (f32[128]{0:T(128)S(1)}, f32[128,2048]{1,0:T(8,128)S(1)}) fusion(bf16[128,1024]{0,1:T(8,128)(2,1)S(1)} %bitcast.59, bf16[1024,2048]{1,0:T(8,128)(2,1)} %param.24, bf16[128,2048]{1,0:T(8,128)(2,1)} %param.17), kind=kOutput, calls=%fused_computation.20 | convolution fusion | flops 538443648 | bytes 6029824 | tf_op jit(solution)/shard_map/dot_general | solution.py:79
  34.1 1.0 copy-done.1
  35.3 6.0 %gather_fusion = bf16[1024,2048]{1,0:T(8,128)(2,1)} fusion(bf16[129,2048]{1,0:T(8,128)(2,1)S(1)} %concatenate.11, s32[1024]{0:T(1024)S(1)} %fusion.32), kind=kCustom, calls=%fused_computation | custom fusion | bytes 8392704 | tf_op jit(solution)/shard_map/gather | solution.py:106
  41.3 96.1 %all_to_all.30 = bf16[32,32,2048]{2,1,0:T(8,128)(2,1)S(1)} all-to-all(bf16[32,32,2048]{2,1,0:T(8,128)(2,1)} %bitcast.55), channel_id=1, replica_groups=mesh['sp'=16,'tp'=2] {'sp','tp'}, dimensions={0} | all-to-all | bytes 8388608 | tf_op jit(solution)/shard_map/all_to_all | solution.py:111
  137.4 2.0 copy-done.4
  139.4 3.7 %fusion.5 = f32[1024,512]{1,0:T(8,128)} fusion(bf16[1024,2048]{1,0:T(8,128)(2,1)S(1)} %bitcast.57, bf16[1,2048,512]{2,1,0:T(8,128)(2,1)S(1)} %copy-done.6), kind=kOutput, calls=%fused_computation.12 | convolution fusion | flops 2147483648 | bytes 8388608 | tf_op jit(solution)/shard_map/dot_general | solution.py:19
  143.1 10.1 %convolution_convert_fusion = bf16[1024,2048]{1,0:T(8,128)(2,1)} fusion(bf16[1,512,2048]{2,1,0:T(8,128)(2,1)S(1)} %copy-done, f32[1024,512]{1,0:T(8,128)} %fusion.5, bf16[1024,2048]{1,0:T(8,128)(2,1)} %bitcast.58, bf16[1,2048,512]{2,1,0:T(8,128)(2,1)} %param.31), kind=kOutput, calls=%fused_computation.4 | convolution fusion | flops 4300210176 | bytes 14680064 | tf_op jit(solution)/shard_map/dot_general | solution.py:21
  153.1 6.1 %all-to-all-start.2 = ((bf16[32,32,2048]{2,1,0:T(8,128)(2,1)}), bf16[32,32,2048]{2,1,0:T(8,128)(2,1)}, u32[]{:S(2)}, u32[]{:S(2)}) async-start(bf16[32,32,2048]{2,1,0:T(8,128)(2,1)} %bitcast.56), calls=%async_computation.2 | async-start | bytes 8388608 | tf_op jit(solution)/shard_map/all_to_all | solution.py:116
  159.4 2.0 fusion.41
  161.5 90.2 %all-to-all-done.2 = bf16[32,32,2048]{2,1,0:T(8,128)(2,1)} async-done(((bf16[32,32,2048]{2,1,0:T(8,128)(2,1)}), bf16[32,32,2048]{2,1,0:T(8,128)(2,1)}, u32[]{:S(2)}, u32[]{:S(2)}) %all-to-all-start.2) | async-done | bytes 4194336 | tf_op jit(solution)/shard_map/all_to_all | solution.py:116
  251.7 8.0 %gather_fusion.1 = bf16[512,2048]{1,0:T(8,128)(2,1)} fusion(bf16[1024,2048]{1,0:T(8,128)(2,1)} %bitcast.17, s32[1024]{0:T(1024)S(1)} %pad_clamp_fusion), kind=kCustom, calls=%fused_computation.1 | custom fusion | bytes 4196352 | tf_op jit(solution)/shard_map/gather | solution.py:117
  259.6 4.8 %reshape.87 = f32[128,4,2048]{2,1,0:T(4,128)} reshape(bf16[512,2048]{1,0:T(8,128)(2,1)} %gather_fusion.1) | data formatting | bytes 6291456 | tf_op jit(solution)/shard_map/convert_element_type | solution.py:119
  264.4 6.4 %multiply_reduce_fusion = f32[128,2048]{1,0:T(8,128)} fusion(f32[128,4,2048]{2,1,0:T(4,128)} %reshape.87, f32[128,4]{1,0:T(8,128)S(1)} %copy.29), kind=kLoop, calls=%fused_computation.3 | loop fusion | flops 1835008 | bytes 5244928 | tf_op jit(solution)/shard_map/reduce_sum | solution.py:122
  270.8 4.3 %fusion.3 = bf16[128,2048]{1,0:T(8,128)(2,1)} fusion(f32[128,2048]{1,0:T(8,128)} %multiply_reduce_fusion, f32[128,2048]{1,0:T(8,128)S(1)} %copy-done.2, bf16[512,2048]{1,0:T(8,128)(2,1)} %param.30, bf16[128,2048]{1,0:T(8,128)(2,1)} %copy-done.3, bf16[2048,512]{1,0:T(8,128)(2,1)} %param.29, f32[128,512]{1,0:T(8,128)S(1)} %fusion.41), kind=kOutput, calls=%fused_computation.10 | convolution fusion | flops 538050560 | bytes 7602176 | tf_op jit(solution)/shard_map/dot_general | solution.py:88
  (47 shorter events, 7.4 us)
Async XLA Ops:
  0.0 143.1 %copy-start = (bf16[1,512,2048]{2,1,0:T(8,128)(2,1)S(1)}, bf16[1,512,2048]{2,1,0:T(8,128)(2,1)}, u32[]{:S(2)}) copy-start(bf16[1,512,2048]{2,1,0:T(8,128)(2,1)} %param.33) | copy-start | bytes 6291460
  0.9 20.0 %collective-permute-start.2 = (bf16[2]{0:T(256)(128)(2,1)S(1)}, bf16[2]{0:T(256)(128)(2,1)S(1)}, u32[]{:S(2)}, u32[]{:S(2)}) collective-permute-start(bf16[2]{0:T(256)(128)(2,1)S(1)} %slice.41), channel_id=1, source_target_pairs={{0,2},{2,4},{4,6},{6,8},{8,10},{10,12},{12,14},{14,16},{16,18},{18... | collective-permute-start | bytes 20 | tf_op jit(solution)/shard_map/ppermute | solution.py:12
  4.7 17.0 %collective-permute-start = (bf16[2,512]{1,0:T(2,128)(2,1)S(1)}, bf16[2,512]{1,0:T(2,128)(2,1)S(1)}, u32[]{:S(2)}, u32[]{:S(2)}) collective-permute-start(bf16[2,512]{1,0:T(2,128)(2,1)S(1)} %slice.38), channel_id=1, source_target_pairs={{0,2},{2,4},{4,6},{6,8},{8,10},{10,12},{12,14},{14,16},{16,18},{18... | collective-permute-start | bytes 6152 | tf_op jit(solution)/shard_map/ppermute | solution.py:12
  8.6 13.2 %collective-permute-start.1 = (bf16[2,512]{1,0:T(2,128)(2,1)S(1)}, bf16[2,512]{1,0:T(2,128)(2,1)S(1)}, u32[]{:S(2)}, u32[]{:S(2)}) collective-permute-start(bf16[2,512]{1,0:T(2,128)(2,1)S(1)} %slice.39), channel_id=1, source_target_pairs={{0,2},{2,4},{4,6},{6,8},{8,10},{10,12},{12,14},{14,16},{16,18},{18... | collective-permute-start | bytes 6152 | tf_op jit(solution)/shard_map/ppermute | solution.py:12
  34.1 1.0 copy-start.1
  35.2 124.2 %copy-start.3 = (bf16[128,2048]{1,0:T(8,128)(2,1)}, bf16[128,2048]{1,0:T(8,128)(2,1)S(1)}, u32[]{:S(2)}) copy-start(bf16[128,2048]{1,0:T(8,128)(2,1)S(1)} %multiply_convert_fusion.1) | copy-start | bytes 1572868
  41.3 98.0 %copy-start.6 = (bf16[1,2048,512]{2,1,0:T(8,128)(2,1)S(1)}, bf16[1,2048,512]{2,1,0:T(8,128)(2,1)}, u32[]{:S(2)}) copy-start(bf16[1,2048,512]{2,1,0:T(8,128)(2,1)} %param.32) | copy-start | bytes 6291460
  137.4 2.0 copy-start.4
  153.1 6.1 %copy-start.5 = (f32[128,4]{0,1:T(4,128)S(1)}, f32[128,4]{0,1:T(4,128)}, u32[]{:S(2)}) copy-start(f32[128,4]{0,1:T(4,128)} %param.27) | copy-start | bytes 6148
  153.1 98.6 %all-to-all-start.2 = ((bf16[32,32,2048]{2,1,0:T(8,128)(2,1)}), bf16[32,32,2048]{2,1,0:T(8,128)(2,1)}, u32[]{:S(2)}, u32[]{:S(2)}) async-start(bf16[32,32,2048]{2,1,0:T(8,128)(2,1)} %bitcast.56), calls=%async_computation.2 | async-start | bytes 8388608 | tf_op jit(solution)/shard_map/all_to_all | solution.py:116
  264.4 6.4 %copy-start.2 = (f32[128,2048]{1,0:T(8,128)S(1)}, f32[128,2048]{1,0:T(8,128)}, u32[]{:S(2)}) copy-start(f32[128,2048]{1,0:T(8,128)} %copy-done.1) | copy-start | bytes 3145732
where the time goes:
time: 279 us; the launch traced here: 275 us
  blocking collectives  104 us (37%)
  waiting for transfers between devices  90.2 us (32%)
  local copies, waits for them, and re-layouts  27.4 us (10%)
  matrix products  23.2 us (8%)
  starting transfers between devices  15.5 us (6%)
  other arithmetic  15 us (5%)
    all_to_all x1, blocking collectives, shards(): lax.all_to_all(outgoing, ('sp', 'tp'), split_axis=0, concat_axis=0, tiled...  96.1 us
    all_to_all x1, waiting for transfers between devices, shards(): lax.all_to_all(result, ('sp', 'tp'), split_axis=0, concat_axis=0, tiled=T...  90.2 us
    dot_general x1, matrix products, expert_apply(): jnp.dot(hidden, down_w, preferred_element_type=jnp.float32)  10.1 us
    ppermute x3, starting transfers between devices, from_behind(): return lax.ppermute(value, axis, pairs)  9.32 us
    gather x1, local copies, waits for them, and re-layouts, shards(): returned.reshape(expert_count * capacity, model_width)[slot_of]  7.96 us
    reduce_sum x1, other arithmetic, shards(): routed = jnp.sum(weighted, axis=1)  6.41 us
    all_to_all x1, starting transfers between devices, shards(): lax.all_to_all(result, ('sp', 'tp'), split_axis=0, concat_axis=0, tiled=T...  6.13 us
    gather x1, local copies, waits for them, and re-layouts, shards(): padded_in[slot_source].reshape(expert_count, capacity, model_width)  6.02 us
  transfers between devices with their start and end apart: 4, of which 1 were waited for; matrix products, arithmetic and copies ran while one was open for 5% of the time, Pallas kernels for 0%

commit v1 on v0

v1 whole, which is shorter than its diff:
```python
import functools

import jax
import jax.numpy as jnp
from jax import lax
from jax.experimental import pallas as pl
from jax.experimental.pallas import tpu as pltpu
from jax.sharding import PartitionSpec as P

norm_eps = 1e-06
MESH = pl.DeviceIdType.MESH
F32, BF16 = jnp.float32, jnp.bfloat16


def column_length(seq_devices):
    length = 1
    while length**3 < seq_devices:
        length *= 2
    return length


def from_behind(value, axis, by):
    peers = lax.axis_size(axis)
    pairs = [(i, i + by) for i in range(peers) if 0 <= i + by < peers]
    return lax.ppermute(value, axis, pairs)


def dot(a, b, contract=((1,), (0,))):
    return lax.dot_general(a, b, (contract, ((), ())), preferred_element_type=F32)


def experts_kernel(
    nz,
    plane,
    cores,
    slots,
    tops,
    x_hbm,
    meta_hbm,
    mid_hbm,
    sg_hbm,
    su_hbm,
    sd_hbm,
    eg_hbm,
    eu_hbm,
    ed_hbm,
    out_ref,
    gath,
    gmeta,
    sbuf,
    rbuf,
    res,
    back,
    zout,
    zin,
    acc,
    mid,
    sg,
    su,
    sd,
    eg,
    eu,
    ed,
    load_sem,
    own_send,
    own_meta_send,
    fwd_send,
    fwd_meta_send,
    z_recv,
    z_meta_recv,
    d_send,
    d_recv,
    b_send,
    b_recv,
    r_send,
    r_recv,
):
    me_sp, me_tp = lax.axis_index("sp"), lax.axis_index("tp")
    peers = plane * cores
    me_z, me_p = me_sp // plane, me_sp % plane
    me_q = me_p * cores + me_tp
    width = x_hbm.shape[1]

    def plane_dev(q):
        return (me_z * plane + q // cores, q % cores)

    def column_dev(z):
        return (z * plane + me_p, me_tp)

    loads = [
        pltpu.make_async_copy(src, dst, load_sem.at[i])
        for i, (src, dst) in enumerate(
            [
                (x_hbm, gath.at[me_z]),
                (meta_hbm, gmeta.at[me_z]),
                (mid_hbm, mid),
                (sg_hbm, sg),
                (su_hbm, su),
                (sd_hbm, sd),
                (eg_hbm, eg),
                (eu_hbm, eu),
                (ed_hbm, ed),
            ]
        )
    ]
    for load in loads:
        load.start()

    barrier = pltpu.get_barrier_semaphore()

    def greet_column(r, carry):
        pl.semaphore_signal(
            barrier, inc=1, device_id=column_dev((me_z + r) % nz), device_id_type=MESH
        )
        return carry

    def greet_plane(j, carry):
        pl.semaphore_signal(
            barrier, inc=1, device_id=plane_dev((me_q + j) % peers), device_id_type=MESH
        )
        return carry

    lax.fori_loop(1, nz, greet_column, 0)
    lax.fori_loop(1, peers, greet_plane, 0)
    pl.semaphore_wait(barrier, nz - 1 + peers - 1)

    def block_of(r):
        fewer = jnp.minimum(me_z, nz - 1 - me_z)
        paired = r <= 2 * fewer
        apart = jnp.where(paired, (r + 1) // 2, r - fewer)
        lower = jnp.where(paired, r % 2, jnp.where(me_z > nz - 1 - me_z, 1, 0))
        return jnp.where(lower == 1, me_z - apart, me_z + apart), lower

    def hop(z, target, send, meta_send):
        return (
            pltpu.make_async_remote_copy(
                gmeta.at[z], gmeta.at[z], meta_send, z_meta_recv.at[z], column_dev(target), MESH
            ),
            pltpu.make_async_remote_copy(
                gath.at[z], gath.at[z], send, z_recv.at[z], column_dev(target), MESH
            ),
        )

    loads[0].wait()
    loads[1].wait()

    def own_hops(act):
        @pl.when(me_z > 0)
        def _():
            for copy in hop(me_z, me_z - 1, own_send.at[0], own_meta_send.at[0]):
                act(copy)

        @pl.when(me_z < nz - 1)
        def _():
            for copy in hop(me_z, me_z + 1, own_send.at[1], own_meta_send.at[1]):
                act(copy)

    def forward_hops(r, act):
        z, lower = block_of(r)

        @pl.when((lower == 1) & (me_z < nz - 1))
        def _():
            for copy in hop(z, me_z + 1, fwd_send.at[r], fwd_meta_send.at[r]):
                act(copy)

        @pl.when((lower == 0) & (me_z > 0))
        def _():
            for copy in hop(z, me_z - 1, fwd_send.at[r], fwd_meta_send.at[r]):
                act(copy)

    own_hops(lambda copy: copy.start())

    def slot_match(z, k):
        first = me_z * peers * slots
        places = lax.broadcasted_iota(jnp.int32, (peers * slots, gmeta.shape[2]), 0) + first
        return places.astype(F32) == gmeta[z, k : k + 1, :]

    def out_copy(r, j):
        q = (me_q + j) % peers
        return pltpu.make_async_remote_copy(
            sbuf.at[r, q], rbuf.at[r, me_q], d_send.at[r, j], d_recv.at[r, j], plane_dev(q), MESH
        )

    def back_copy(r, j):
        q = (me_q + j) % peers
        return pltpu.make_async_remote_copy(
            res.at[r, q], back.at[r, me_q], b_send.at[r, j], b_recv.at[r, j], plane_dev(q), MESH
        )

    def return_copy(r):
        z, _ = block_of(r)
        return pltpu.make_async_remote_copy(
            zout.at[r], zin.at[me_z], r_send.at[r], r_recv.at[me_z], column_dev(z), MESH
        )

    def over_peers(act):
        def step(j, carry):
            act(j)
            return carry

        lax.fori_loop(1, peers, step, 0)

    def dispatch(r):
        z, _ = block_of(r)

        @pl.when(r > 0)
        def _():
            for copy in hop(z, me_z, fwd_send.at[r], fwd_meta_send.at[r]):
                copy.wait_recv()
            forward_hops(r, lambda copy: copy.start())

        pick = jnp.zeros((peers * slots, gmeta.shape[2]), F32)
        for k in range(tops):
            pick = jnp.where(slot_match(z, k), 1.0, pick)
        rows = dot(pick.astype(BF16), gath[z]).astype(BF16)
        sbuf[r] = rows.reshape(peers, slots, width)
        rbuf[r, me_q] = sbuf[r, me_q]
        over_peers(lambda j: out_copy(r, j).start())

    def apply(r):
        over_peers(lambda j: out_copy(r, j).wait_recv())
        rows = rbuf[r].reshape(peers * slots, width)
        gate = dot(rows, eg[0])
        hidden = (gate / (1.0 + jnp.exp(-gate)) * dot(rows, eu[0])).astype(BF16)
        res[r] = dot(hidden, ed[0]).astype(BF16).reshape(peers, slots, width)
        back[r, me_q] = res[r, me_q]
        over_peers(lambda j: back_copy(r, j).start())

    def collect(r):
        over_peers(lambda j: back_copy(r, j).wait_recv())
        z, _ = block_of(r)
        weight = jnp.zeros((peers * slots, gmeta.shape[2]), F32)
        for k in range(tops):
            weight = jnp.where(slot_match(z, k), gmeta[z, tops + k : tops + k + 1, :], weight)
        rows = back[r].reshape(peers * slots, width)
        total = dot(weight.astype(BF16), rows, ((0,), (0,)))

        @pl.when(r == 0)
        def _():
            acc[...] += total

        @pl.when(r > 0)
        def _():
            zout[r] = total.astype(BF16)
            return_copy(r).start()

    def step(i, carry):
        @pl.when(i < nz)
        def _():
            dispatch(i)

        @pl.when(i == 0)
        def _():
            for load in loads[2:6]:
                load.wait()
            rows = gath[me_z]
            gate = dot(rows, sg[...])
            hidden = (gate / (1.0 + jnp.exp(-gate)) * dot(rows, su[...])).astype(BF16)
            acc[...] = mid[...].astype(F32) + dot(hidden, sd[...])
            for load in loads[6:]:
                load.wait()

        @pl.when((i >= 1) & (i <= nz))
        def _():
            apply(i - 1)

        @pl.when(i >= 2)
        def _():
            collect(i - 2)

        return carry

    lax.fori_loop(0, nz + 2, step, 0)

    def settle(r, carry):
        z, _ = block_of(r)
        pltpu.make_async_remote_copy(
            zout.at[r], zin.at[z], r_send.at[r], r_recv.at[z], column_dev(z), MESH
        ).wait_recv()
        acc[...] += zin[z].astype(F32)
        return carry

    lax.fori_loop(1, nz, settle, 0)
    out_ref[...] = acc[...].astype(BF16)

    own_hops(lambda copy: copy.wait_send())

    def drain_column(r, carry):
        forward_hops(r, lambda copy: copy.wait_send())
        return_copy(r).wait_send()
        return carry

    lax.fori_loop(1, nz, drain_column, 0)

    def drain_plane(r, carry):
        over_peers(lambda j: out_copy(r, j).wait_send())
        over_peers(lambda j: back_copy(r, j).wait_send())
        return carry

    lax.fori_loop(0, nz, drain_plane, 0)


def run_experts(ffn_in, meta, middle, shared, routed, slots):
    rows, width = ffn_in.shape
    seq_devices, cores = lax.axis_size("sp"), lax.axis_size("tp")
    nz = column_length(seq_devices)
    plane = seq_devices // nz
    peers = plane * cores
    dma = pltpu.SemaphoreType.DMA
    tile = (nz, peers, slots, width)
    hbm = pl.BlockSpec(memory_space=pl.ANY)
    weights = [pltpu.VMEM(w.shape, w.dtype) for w in (*shared, *routed)]
    return pl.pallas_call(
        functools.partial(experts_kernel, nz, plane, cores, slots, meta.shape[0] // 2),
        out_shape=jax.ShapeDtypeStruct((rows, width), BF16),
        in_specs=[hbm] * 9,
        out_specs=pl.BlockSpec(memory_space=pltpu.VMEM),
        scratch_shapes=[
            pltpu.VMEM((nz, rows, width), BF16),
            pltpu.VMEM((nz, *meta.shape), F32),
            pltpu.VMEM(tile, BF16),
            pltpu.VMEM(tile, BF16),
            pltpu.VMEM(tile, BF16),
            pltpu.VMEM(tile, BF16),
            pltpu.VMEM((nz, rows, width), BF16),
            pltpu.VMEM((nz, rows, width), BF16),
            pltpu.VMEM((rows, width), F32),
            pltpu.VMEM((rows, width), BF16),
            *weights,
            dma((9,)),
            dma((2,)),
            dma((2,)),
            dma((nz,)),
            dma((nz,)),
            dma((nz,)),
            dma((nz,)),
            dma((nz, peers)),
            dma((nz, peers)),
            dma((nz, peers)),
            dma((nz, peers)),
            dma((nz,)),
            dma((nz,)),
        ],
        compiler_params=pltpu.CompilerParams(
            collective_id=0, has_side_effects=True, vmem_limit_bytes=67043328
        ),
    )(ffn_in, meta, middle, *shared, *routed)


def shards(
    residual,
    outer_gate,
    conv_input,
    conv_value,
    doc_ids,
    conv_taps,
    branch_gain,
    out_weight,
    ffn_gain,
    route_ids,
    route_weight,
    shared_gate,
    shared_up,
    shared_down,
    expert_gate,
    expert_up,
    expert_down,
):
    seq_rows = conv_input.shape[0]
    half_width = conv_input.shape[1]
    tap_count = conv_taps.shape[0]
    lead_rows = tap_count - 1
    doc_float = doc_ids.astype(jnp.float32)
    prev_input, prev_value, prev_doc = from_behind(
        (
            conv_input[seq_rows - lead_rows :],
            conv_value[seq_rows - lead_rows :],
            doc_float[seq_rows - lead_rows :].astype(jnp.bfloat16),
        ),
        "sp",
        1,
    )
    source = jnp.concatenate(
        [
            prev_input.astype(jnp.float32) * prev_value.astype(jnp.float32),
            conv_input.astype(jnp.float32) * conv_value.astype(jnp.float32),
        ],
        axis=0,
    )
    doc_extended = jnp.concatenate([prev_doc.astype(jnp.float32), doc_float], axis=0)
    mixed_conv = jnp.zeros((seq_rows, half_width), jnp.float32)
    for tap in range(tap_count):
        same_doc = (doc_extended[tap : tap + seq_rows] == doc_float).astype(jnp.float32)[:, None]
        mixed_conv = (
            mixed_conv
            + conv_taps[tap].astype(jnp.float32)[None, :] * source[tap : tap + seq_rows] * same_doc
        )
    branch = outer_gate.astype(jnp.float32) * mixed_conv
    square_total = lax.psum(jnp.sum(branch * branch, axis=1, keepdims=True), "tp")
    inv_rms = lax.rsqrt(square_total / (half_width * lax.axis_size("tp")) + norm_eps)
    normed = (branch * inv_rms * branch_gain.astype(jnp.float32)[None, :]).astype(jnp.bfloat16)
    local_rows = residual.shape[0]
    token_rows = lax.all_to_all(normed, "tp", split_axis=0, concat_axis=1, tiled=True)
    update = jnp.dot(token_rows, out_weight, preferred_element_type=jnp.float32)
    middle = (residual.astype(jnp.float32) + update).astype(jnp.bfloat16)
    mid_float = middle.astype(jnp.float32)
    mid_rms = lax.rsqrt(jnp.mean(mid_float * mid_float, axis=1, keepdims=True) + norm_eps)
    ffn_in = (mid_float * mid_rms * ffn_gain.astype(jnp.float32)[None, :]).astype(jnp.bfloat16)

    top_count = route_ids.shape[1]
    core_devices = lax.axis_size("tp")
    expert_count = lax.axis_size("sp") * core_devices
    capacity = local_rows * core_devices * top_count // expert_count
    slots = -(-capacity // 16) * 16
    ids = route_ids.T
    experts = jnp.arange(expert_count, dtype=jnp.int32)
    named = jnp.sum((ids[:, None, :] == experts[None, :, None]).astype(F32), axis=0)
    token = jnp.arange(local_rows, dtype=jnp.int32)
    before = (token[:, None] < token[None, :]).astype(BF16)
    earlier = jnp.dot(named.astype(BF16), before, preferred_element_type=F32)
    rank = jnp.sum(
        jnp.where(ids[:, None, :] == experts[None, :, None], earlier[None, :, :], 0.0), axis=1
    )
    places = ids.astype(F32) * slots + rank
    meta = jnp.concatenate([places, route_weight.T], axis=0)
    return run_experts(
        ffn_in,
        meta,
        middle,
        (shared_gate, shared_up, shared_down),
        (expert_gate, expert_up, expert_down),
        slots,
    )


def solution(mesh):
    placed = (
        P(("sp", "tp"), None),
        P("sp", "tp"),
        P("sp", "tp"),
        P("sp", "tp"),
        P("sp"),
        P(None, "tp"),
        P("tp"),
        P(),
        P(),
        P(("sp", "tp"), None),
        P(("sp", "tp"), None),
        P(),
        P(),
        P(),
        P(("sp", "tp"), None, None),
        P(("sp", "tp"), None, None),
        P(("sp", "tp"), None, None),
    )
    return jax.shard_map(
        shards, mesh=mesh, in_specs=placed, out_specs=P(("sp", "tp"), None), check_vma=False
    )
```

time: 279 us -> 169 us (0.61); the launches traced: 275 us -> 169 us
  Pallas kernels: 0 us -> 133 us
  blocking collectives: 104 us -> 7.56 us
  waiting for transfers between devices: 90.2 us -> 0.01 us
  local copies, waits for them, and re-layouts: 27.4 us -> 4.32 us
  matrix products: 23.2 us -> 3.17 us
  starting transfers between devices: 15.5 us -> 9.45 us
  other arithmetic: 15 us -> 10.6 us
    pallas_call x0 -> x1, Pallas kernels: none -> 133 us  [run_experts(): pl.pallas_call(functools.partial(experts_kernel, nz, plane, cores, slots,...]
    all_to_all x1 -> x0, blocking collectives: 96.1 us -> none  [shards(): lax.all_to_all(outgoing, ('sp', 'tp'), split_axis=0, concat_axis=0, tiled...]
    all_to_all x1 -> x0, waiting for transfers between devices: 90.2 us -> none  [shards(): lax.all_to_all(result, ('sp', 'tp'), split_axis=0, concat_axis=0, tiled=T...]
    dot_general x4 -> x1, matrix products: 20.1 us -> 0.14 us  [shards(): earlier = jnp.dot(named.astype(BF16), before, preferred_element_type=F32)]
    gather x2 -> x0, local copies, waits for them, and re-layouts: 14 us -> none  [the longest x1 7.96 us: shards(): returned.reshape(expert_count * capacity, model_width)[slot_of]]
    all_to_all x1 -> x0, starting transfers between devices: 6.13 us -> none  [shards(): lax.all_to_all(result, ('sp', 'tp'), split_axis=0, concat_axis=0, tiled=T...]
    reduce_sum x2, other arithmetic: 6.51 us -> 1.4 us  [the longest x1 0.71 us: shards(): jnp.sum(jnp.where(ids[:, None, :] == experts[None, :, None], earlier[None...]
    convert_element_type x1 -> x0, local copies, waits for them, and re-layouts: 4.75 us -> none  [shards(): returned_rows.astype(jnp.float32)]
  transfers between devices with their start and end apart: 4 -> 3, of which waited for: 1 -> 0; matrix products, arithmetic and copies ran while one was open for 5% -> 5% of each run, Pallas kernels for 0% -> 0%
where the time goes in v1:
time: 169 us
  Pallas kernels  133 us (79%)
  other arithmetic  10.6 us (6%)
  starting transfers between devices  9.45 us (6%)
  blocking collectives  7.56 us (4%)
  local copies, waits for them, and re-layouts  4.32 us (3%)
  matrix products  3.17 us (2%)
    pallas_call x1, Pallas kernels, run_experts(): pl.pallas_call(functools.partial(experts_kernel, nz, plane, cores, slots,...  133 us
    ppermute x3, starting transfers between devices, from_behind(): return lax.ppermute(value, axis, pairs)  9.45 us
    all_to_all x1, blocking collectives, shards(): lax.all_to_all(normed, 'tp', split_axis=0, concat_axis=1, tiled=True)  3.92 us
    psum x1, blocking collectives, shards(): lax.psum(jnp.sum(branch * branch, axis=1, keepdims=True), 'tp')  3.64 us
  transfers between devices with their start and end apart: 3, of which 0 were waited for; matrix products, arithmetic and copies ran while one was open for 5% of the time, Pallas kernels for 0%

profile of v1, /device:TPU:25, one launch (start us, length us, event | category | flops | bytes accessed | tf_op | source)
XLA Modules:
  0.0 168.6 jit_solution(11639903990556128651)
XLA Ops:
  0.0 0.7 convert_convert_fusion
  0.8 3.1 %collective-permute-start.2 = (bf16[2]{0:T(256)(128)(2,1)S(1)}, bf16[2]{0:T(256)(128)(2,1)S(1)}, u32[]{:S(2)}, u32[]{:S(2)}) collective-permute-start(bf16[2]{0:T(256)(128)(2,1)S(1)} %slice.35), channel_id=1, source_target_pairs={{0,2},{2,4},{4,6},{6,8},{8,10},{10,12},{12,14},{14,16},{16,18},{18... | collective-permute-start | bytes 20 | tf_op jit(solution)/shard_map/ppermute | solution.py:25
  3.9 0.7 slice.33
  4.6 3.1 %collective-permute-start.1 = (bf16[2,512]{1,0:T(2,128)(2,1)S(1)}, bf16[2,512]{1,0:T(2,128)(2,1)S(1)}, u32[]{:S(2)}, u32[]{:S(2)}) collective-permute-start(bf16[2,512]{1,0:T(2,128)(2,1)S(1)} %slice.33), channel_id=1, source_target_pairs={{0,2},{2,4},{4,6},{6,8},{8,10},{10,12},{12,14},{14,16},{16,18},{18... | collective-permute-start | bytes 6152 | tf_op jit(solution)/shard_map/ppermute | solution.py:25
  7.7 0.7 slice.32
  8.4 3.2 %collective-permute-start = (bf16[2,512]{1,0:T(2,128)(2,1)S(1)}, bf16[2,512]{1,0:T(2,128)(2,1)S(1)}, u32[]{:S(2)}, u32[]{:S(2)}) collective-permute-start(bf16[2,512]{1,0:T(2,128)(2,1)S(1)} %slice.32), channel_id=1, source_target_pairs={{0,2},{2,4},{4,6},{6,8},{8,10},{10,12},{12,14},{14,16},{16,18},{18... | collective-permute-start | bytes 6152 | tf_op jit(solution)/shard_map/ppermute | solution.py:25
  11.7 1.1 convert_multiply_fusion.2
  12.8 0.7 convert_element_type.79
  13.4 0.8 slice_convert_fusion.2
  14.2 0.7 convert_element_type.83
  14.9 0.7 convert_reduce_fusion
  15.8 0.7 select_reduce_fusion
  16.5 0.7 multiply_add_fusion
  17.2 1.3 pad_maximum_fusion.1.meta_hbm
  18.5 0.8 compare_convert_fusion.2
  19.3 1.3 multiply_reduce_fusion
  20.6 3.6 %psum.7 = f32[256,1]{0,1:T(1,128)S(1)} all-reduce(f32[256,1]{0,1:T(1,128)S(1)} %bitcast.23), channel_id=1, replica_groups=mesh['sp'=16,'tp'=2] {'tp'}, use_global_device_ids=true, to_apply=%region_1.0 | all-reduce | flops 256 | bytes 2048 | tf_op jit(solution)/shard_map/psum | solution.py:399
  24.4 3.9 %all_to_all.19 = bf16[2,128,512]{2,1,0:T(8,128)(2,1)S(1)} all-to-all(bf16[2,128,512]{2,1,0:T(8,128)(2,1)S(1)} %bitcast.15), channel_id=1, replica_groups=mesh['sp'=16,'tp'=2] {'tp'}, dimensions={0} | all-to-all | bytes 524288 | tf_op jit(solution)/shard_map/all_to_all | solution.py:403
  28.3 0.2 copy.19
  28.5 3.0 %fusion.1 = (f32[128]{0:T(128)S(1)}, bf16[128,2048]{1,0:T(8,128)(2,1)S(1)}) fusion(bf16[128,1024]{0,1:T(8,128)(2,1)S(1)} %bitcast.14, bf16[1024,2048]{1,0:T(8,128)(2,1)} %param.24, bf16[128,2048]{1,0:T(8,128)(2,1)S(1)} %copy-done.1), kind=kOutput, calls=%fused_computation.4 | convolution fusion | flops 538443648 | bytes 5505536 | tf_op jit(solution)/shard_map/dot_general | solution.py:404
  31.6 0.8 copy-done
  32.3 1.0 fusion.3.x_hbm
  33.3 133.3 %shard_map.163 = bf16[128,2048]{1,0:T(8,128)(2,1)} custom-call(bf16[128,2048]{1,0:T(8,128)(2,1)} %fusion.3.x_hbm, f32[8,128]{1,0:T(8,128)} %pad_maximum_fusion.1.meta_hbm, bf16[128,2048]{1,0:T(8,128)(2,1)} %copy-done, bf16[2048,512]{1,0:T(8,128)(2,1)} %sg_hbm.1, bf16[2048,512]{1,0:T(8,128)(2,1)} %su_hbm.1, bf16[512,2048]{1,0:T(8,128)(2,1)} %sd_hbm.1, ...), custom_call_target="tpu_custom_call" | custom-call | tf_op jit(solution)/shard_map/pallas_call | solution.py:313
  166.7 1.9 %copy.21 = bf16[128,2048]{1,0:T(8,128)(2,1)} copy(bf16[128,2048]{1,0:T(8,128)(2,1)} %shard_map.163) | data formatting | bytes 1048576
  (14 shorter events, 0.4 us)
Async XLA Ops:
  0.8 17.7 %collective-permute-start.2 = (bf16[2]{0:T(256)(128)(2,1)S(1)}, bf16[2]{0:T(256)(128)(2,1)S(1)}, u32[]{:S(2)}, u32[]{:S(2)}) collective-permute-start(bf16[2]{0:T(256)(128)(2,1)S(1)} %slice.35), channel_id=1, source_target_pairs={{0,2},{2,4},{4,6},{6,8},{8,10},{10,12},{12,14},{14,16},{16,18},{18... | collective-permute-start | bytes 20 | tf_op jit(solution)/shard_map/ppermute | solution.py:25
  4.6 14.7 %collective-permute-start.1 = (bf16[2,512]{1,0:T(2,128)(2,1)S(1)}, bf16[2,512]{1,0:T(2,128)(2,1)S(1)}, u32[]{:S(2)}, u32[]{:S(2)}) collective-permute-start(bf16[2,512]{1,0:T(2,128)(2,1)S(1)} %slice.33), channel_id=1, source_target_pairs={{0,2},{2,4},{4,6},{6,8},{8,10},{10,12},{12,14},{14,16},{16,18},{18... | collective-permute-start | bytes 6152 | tf_op jit(solution)/shard_map/ppermute | solution.py:25
  8.4 20.1 %copy-start.1 = (bf16[128,2048]{1,0:T(8,128)(2,1)S(1)}, bf16[128,2048]{1,0:T(8,128)(2,1)}, u32[]{:S(2)}) copy-start(bf16[128,2048]{1,0:T(8,128)(2,1)} %param.17) | copy-start | bytes 1572868
  8.4 10.9 %collective-permute-start = (bf16[2,512]{1,0:T(2,128)(2,1)S(1)}, bf16[2,512]{1,0:T(2,128)(2,1)S(1)}, u32[]{:S(2)}, u32[]{:S(2)}) collective-permute-start(bf16[2,512]{1,0:T(2,128)(2,1)S(1)} %slice.32), channel_id=1, source_target_pairs={{0,2},{2,4},{4,6},{6,8},{8,10},{10,12},{12,14},{14,16},{16,18},{18... | collective-permute-start | bytes 6152 | tf_op jit(solution)/shard_map/ppermute | solution.py:25
  31.5 0.8 copy-start

commit v2 on v1

--- a/solution.py
+++ b/solution.py
@@ -19,12 +19,6 @@
     return length
 
 
-def from_behind(value, axis, by):
-    peers = lax.axis_size(axis)
-    pairs = [(i, i + by) for i in range(peers) if 0 <= i + by < peers]
-    return lax.ppermute(value, axis, pairs)
-
-
 def dot(a, b, contract=((1,), (0,))):
     return lax.dot_general(a, b, (contract, ((), ())), preferred_element_type=F32)
 
@@ -35,16 +29,39 @@
     cores,
     slots,
     tops,
-    x_hbm,
-    meta_hbm,
-    mid_hbm,
+    expert_count,
+    in_hbm,
+    val_hbm,
+    doc_hbm,
+    route_hbm,
+    outer_hbm,
+    ow_hbm,
+    residual_hbm,
     sg_hbm,
     su_hbm,
     sd_hbm,
     eg_hbm,
     eu_hbm,
     ed_hbm,
+    taps_ref,
+    branch_gain_ref,
+    ffn_gain_ref,
     out_ref,
+    conv_in,
+    conv_val,
+    docs,
+    route,
+    outer,
+    ow,
+    residual,
+    source,
+    halo_in,
+    halo_val,
+    halo_doc,
+    scaled,
+    squares,
+    other_scaled,
+    other_squares,
     gath,
     gmeta,
     sbuf,
@@ -54,7 +71,6 @@
     zout,
     zin,
     acc,
-    mid,
     sg,
     su,
     sd,
@@ -62,6 +78,10 @@
     eu,
     ed,
     load_sem,
+    halo_send,
+    halo_recv,
+    half_send,
+    half_recv,
     own_send,
     own_meta_send,
     fwd_send,
@@ -79,7 +99,8 @@
     peers = plane * cores
     me_z, me_p = me_sp // plane, me_sp % plane
     me_q = me_p * cores + me_tp
-    width = x_hbm.shape[1]
+    width = residual.shape[1]
+    seq_devices = nz * plane
 
     def plane_dev(q):
         return (me_z * plane + q // cores, q % cores)
@@ -91,9 +112,13 @@
         pltpu.make_async_copy(src, dst, load_sem.at[i])
         for i, (src, dst) in enumerate(
             [
-                (x_hbm, gath.at[me_z]),
-                (meta_hbm, gmeta.at[me_z]),
-                (mid_hbm, mid),
+                (in_hbm, conv_in),
+                (val_hbm, conv_val),
+                (doc_hbm, docs),
+                (route_hbm, route),
+                (outer_hbm, outer),
+                (ow_hbm, ow),
+                (residual_hbm, residual),
                 (sg_hbm, sg),
                 (su_hbm, su),
                 (sd_hbm, sd),
@@ -122,7 +147,100 @@
 
     lax.fori_loop(1, nz, greet_column, 0)
     lax.fori_loop(1, peers, greet_plane, 0)
-    pl.semaphore_wait(barrier, nz - 1 + peers - 1)
+    ahead = ((me_sp + 1) % seq_devices, me_tp)
+    behind = ((me_sp + seq_devices - 1) % seq_devices, me_tp)
+    pl.semaphore_signal(barrier, inc=1, device_id=ahead, device_id_type=MESH)
+    pl.semaphore_signal(barrier, inc=1, device_id=behind, device_id_type=MESH)
+    for load in loads[:4]:
+        load.wait()
+    pl.semaphore_wait(barrier, nz - 1 + peers - 1 + 2)
+
+    seq_rows, half_width = conv_in.shape
+    lead, packed = halo_doc.shape[0], halo_in.shape[0]
+    halo_copies = [
+        pltpu.make_async_remote_copy(
+            src.at[pl.ds(seq_rows - dst.shape[0], dst.shape[0])],
+            dst,
+            halo_send.at[i],
+            halo_recv.at[i],
+            ahead,
+            MESH,
+        )
+        for i, (src, dst) in enumerate(
+            [(conv_in, halo_in), (conv_val, halo_val), (docs, halo_doc)]
+        )
+    ]
+    for copy in halo_copies:
+        copy.start()
+
+    rows_here = residual.shape[0]
+    named_by = route[...].T
+    experts = lax.broadcasted_iota(jnp.int32, (expert_count, rows_here), 0).astype(F32)
+    matches = [experts == named_by[k : k + 1, :] for k in range(tops)]
+    named = jnp.zeros((expert_count, rows_here), F32)
+    for match in matches:
+        named = jnp.where(match, 1.0, named)
+    square = (rows_here, rows_here)
+    before = lax.broadcasted_iota(jnp.int32, square, 0) < lax.broadcasted_iota(jnp.int32, square, 1)
+    earlier = dot(named.astype(BF16), jnp.where(before, 1.0, 0.0).astype(BF16))
+    for k, match in enumerate(matches):
+        rank = jnp.sum(jnp.where(match, earlier, 0.0), axis=0, keepdims=True)
+        gmeta[me_z, k : k + 1, :] = named_by[k : k + 1, :] * slots + rank
+        gmeta[me_z, tops + k : tops + k + 1, :] = named_by[tops + k : tops + k + 1, :]
+
+    source[lead:, :] = conv_in[...].astype(F32) * conv_val[...].astype(F32)
+    for load in loads[4:7]:
+        load.wait()
+    for copy in halo_copies:
+        copy.wait_recv()
+    inner = me_sp > 0
+    product = halo_in[...].astype(F32) * halo_val[...].astype(F32)
+    source[:lead, :] = jnp.where(inner, product[packed - lead :, :], 0.0)
+    doc_here = docs[...]
+    doc_all = jnp.concatenate([jnp.where(inner, halo_doc[...], -1.0), doc_here], axis=0)
+    tap_count = taps_ref.shape[0]
+    lanes = docs.shape[1]
+    same = []
+    for tap in range(tap_count):
+        first = lead - (tap_count - 1 - tap)
+        same.append(doc_all[first : first + seq_rows, :] == doc_here)
+    total_square = jnp.zeros((seq_rows, 1), F32)
+    for column in range(0, half_width, lanes):
+        part = slice(column, column + lanes)
+        mixed = jnp.zeros((seq_rows, lanes), F32)
+        for tap in range(tap_count):
+            first = lead - (tap_count - 1 - tap)
+            lagged = source[first : first + seq_rows, part]
+            weight = taps_ref[tap : tap + 1, part].astype(F32)
+            mixed = mixed + jnp.where(same[tap], weight * lagged, 0.0)
+        branch = outer[:, part].astype(F32) * mixed
+        total_square = total_square + jnp.sum(branch * branch, axis=1, keepdims=True)
+        scaled[:, part] = (branch * branch_gain_ref[:, part].astype(F32)).astype(BF16)
+    squares[...] = jnp.broadcast_to(total_square, squares.shape)
+
+    other_tp = 1 - me_tp
+    theirs = pl.ds(pl.multiple_of(other_tp * rows_here, rows_here), rows_here)
+    mine = pl.ds(pl.multiple_of(me_tp * rows_here, rows_here), rows_here)
+    half_copies = [
+        pltpu.make_async_remote_copy(
+            src.at[theirs], dst, half_send.at[i], half_recv.at[i], (me_sp, other_tp), MESH
+        )
+        for i, (src, dst) in enumerate([(scaled, other_scaled), (squares, other_squares)])
+    ]
+    for copy in half_copies:
+        copy.start()
+    my_weight = pl.ds(pl.multiple_of(me_tp * half_width, half_width), half_width)
+    their_weight = pl.ds(pl.multiple_of(other_tp * half_width, half_width), half_width)
+    acc[...] = dot(scaled[mine, :], ow[my_weight, :])
+    for copy in half_copies:
+        copy.wait_recv()
+    square_total = (squares[mine, :] + other_squares[...])[:, :1]
+    inv_rms = lax.rsqrt(square_total / (half_width * cores) + norm_eps)
+    update = (acc[...] + dot(other_scaled[...], ow[their_weight, :])) * inv_rms
+    middle = (residual[...].astype(F32) + update).astype(BF16).astype(F32)
+    mid_rms = lax.rsqrt(jnp.mean(middle * middle, axis=1, keepdims=True) + norm_eps)
+    acc[...] = middle
+    gath[me_z] = (middle * mid_rms * ffn_gain_ref[...].astype(F32)).astype(BF16)
 
     def block_of(r):
         fewer = jnp.minimum(me_z, nz - 1 - me_z)
@@ -141,9 +259,6 @@
             ),
         )
 
-    loads[0].wait()
-    loads[1].wait()
-
     def own_hops(act):
         @pl.when(me_z > 0)
         def _():
@@ -224,7 +339,14 @@
         hidden = (gate / (1.0 + jnp.exp(-gate)) * dot(rows, eu[0])).astype(BF16)
         res[r] = dot(hidden, ed[0]).astype(BF16).reshape(peers, slots, width)
         back[r, me_q] = res[r, me_q]
-        over_peers(lambda j: back_copy(r, j).start())
+
+        @pl.when(r > 0)
+        def _():
+            over_peers(lambda j: back_copy(r, j).start())
+
+        @pl.when(r == nz - 1)
+        def _():
+            over_peers(lambda j: back_copy(0, j).start())
 
     def collect(r):
         over_peers(lambda j: back_copy(r, j).wait_recv())
@@ -251,26 +373,26 @@
 
         @pl.when(i == 0)
         def _():
-            for load in loads[2:6]:
+            for load in loads[7:10]:
                 load.wait()
             rows = gath[me_z]
             gate = dot(rows, sg[...])
             hidden = (gate / (1.0 + jnp.exp(-gate)) * dot(rows, su[...])).astype(BF16)
-            acc[...] = mid[...].astype(F32) + dot(hidden, sd[...])
-            for load in loads[6:]:
+            acc[...] += dot(hidden, sd[...])
+            for load in loads[10:]:
                 load.wait()
 
         @pl.when((i >= 1) & (i <= nz))
         def _():
             apply(i - 1)
 
-        @pl.when(i >= 2)
-        def _():
-            collect(i - 2)
+        @pl.when(i >= 3)
+        def _():
+            collect((i - 2) % nz)
 
         return carry
 
-    lax.fori_loop(0, nz + 2, step, 0)
+    lax.fori_loop(0, nz + 3, step, 0)
 
     def settle(r, carry):
         z, _ = block_of(r)
@@ -283,6 +405,8 @@
     lax.fori_loop(1, nz, settle, 0)
     out_ref[...] = acc[...].astype(BF16)
 
+    for copy in halo_copies + half_copies:
+        copy.wait_send()
     own_hops(lambda copy: copy.wait_send())
 
     def drain_column(r, carry):
@@ -298,53 +422,6 @@
         return carry
 
     lax.fori_loop(0, nz, drain_plane, 0)
-
-
-def run_experts(ffn_in, meta, middle, shared, routed, slots):
-    rows, width = ffn_in.shape
-    seq_devices, cores = lax.axis_size("sp"), lax.axis_size("tp")
-    nz = column_length(seq_devices)
-    plane = seq_devices // nz
-    peers = plane * cores
-    dma = pltpu.SemaphoreType.DMA
-    tile = (nz, peers, slots, width)
-    hbm = pl.BlockSpec(memory_space=pl.ANY)
-    weights = [pltpu.VMEM(w.shape, w.dtype) for w in (*shared, *routed)]
-    return pl.pallas_call(
-        functools.partial(experts_kernel, nz, plane, cores, slots, meta.shape[0] // 2),
-        out_shape=jax.ShapeDtypeStruct((rows, width), BF16),
-        in_specs=[hbm] * 9,
-        out_specs=pl.BlockSpec(memory_space=pltpu.VMEM),
-        scratch_shapes=[
-            pltpu.VMEM((nz, rows, width), BF16),
-            pltpu.VMEM((nz, *meta.shape), F32),
-            pltpu.VMEM(tile, BF16),
-            pltpu.VMEM(tile, BF16),
-            pltpu.VMEM(tile, BF16),
-            pltpu.VMEM(tile, BF16),
-            pltpu.VMEM((nz, rows, width), BF16),
-            pltpu.VMEM((nz, rows, width), BF16),
-            pltpu.VMEM((rows, width), F32),
-            pltpu.VMEM((rows, width), BF16),
-            *weights,
-            dma((9,)),
-            dma((2,)),
-            dma((2,)),
-            dma((nz,)),
-            dma((nz,)),
-            dma((nz,)),
-            dma((nz,)),
-            dma((nz, peers)),
-            dma((nz, peers)),
-            dma((nz, peers)),
-            dma((nz, peers)),
-            dma((nz,)),
-            dma((nz,)),
-        ],
-        compiler_params=pltpu.CompilerParams(
-            collective_id=0, has_side_effects=True, vmem_limit_bytes=67043328
-        ),
-    )(ffn_in, meta, middle, *shared, *routed)
 
 
 def shards(
@@ -366,71 +443,88 @@
     expert_up,
     expert_down,
 ):
-    seq_rows = conv_input.shape[0]
-    half_width = conv_input.shape[1]
-    tap_count = conv_taps.shape[0]
-    lead_rows = tap_count - 1
-    doc_float = doc_ids.astype(jnp.float32)
-    prev_input, prev_value, prev_doc = from_behind(
-        (
-            conv_input[seq_rows - lead_rows :],
-            conv_value[seq_rows - lead_rows :],
-            doc_float[seq_rows - lead_rows :].astype(jnp.bfloat16),
+    rows, width = residual.shape
+    seq_rows, half_width = conv_input.shape
+    tops = route_ids.shape[1]
+    seq_devices, cores = lax.axis_size("sp"), lax.axis_size("tp")
+    nz = column_length(seq_devices)
+    plane = seq_devices // nz
+    peers = plane * cores
+    expert_count = seq_devices * cores
+    capacity = rows * cores * tops // expert_count
+    slots = -(-capacity // 16) * 16
+    lanes = 128
+    docs = jnp.broadcast_to(doc_ids.astype(F32)[:, None], (seq_rows, lanes))
+    route = jnp.concatenate([route_ids.astype(F32), route_weight], axis=1)
+    route = jnp.pad(route, ((0, 0), (0, lanes - 2 * tops)))
+    streamed = (
+        conv_input,
+        conv_value,
+        docs,
+        route,
+        outer_gate,
+        out_weight,
+        residual,
+        shared_gate,
+        shared_up,
+        shared_down,
+        expert_gate,
+        expert_up,
+        expert_down,
+    )
+    held = [pltpu.VMEM(a.shape, a.dtype) for a in streamed]
+    small = (conv_taps, branch_gain[None, :], ffn_gain[None, :])
+    dma = pltpu.SemaphoreType.DMA
+    tile = (nz, peers, slots, width)
+    lead, packed = 8, 16
+    return pl.pallas_call(
+        functools.partial(experts_kernel, nz, plane, cores, slots, tops, expert_count),
+        out_shape=jax.ShapeDtypeStruct((rows, width), BF16),
+        in_specs=[pl.BlockSpec(memory_space=pl.ANY)] * len(streamed)
+        + [pl.BlockSpec(memory_space=pltpu.VMEM)] * len(small),
+        out_specs=pl.BlockSpec(memory_space=pltpu.VMEM),
+        scratch_shapes=[
+            *held[:7],
+            pltpu.VMEM((lead + seq_rows, half_width), F32),
+            pltpu.VMEM((packed, half_width), BF16),
+            pltpu.VMEM((packed, half_width), BF16),
+            pltpu.VMEM((lead, lanes), F32),
+            pltpu.VMEM((seq_rows, half_width), BF16),
+            pltpu.VMEM((seq_rows, lanes), F32),
+            pltpu.VMEM((rows, half_width), BF16),
+            pltpu.VMEM((rows, lanes), F32),
+            pltpu.VMEM((nz, rows, width), BF16),
+            pltpu.VMEM((nz, 2 * tops, rows), F32),
+            pltpu.VMEM(tile, BF16),
+            pltpu.VMEM(tile, BF16),
+            pltpu.VMEM(tile, BF16),
+            pltpu.VMEM(tile, BF16),
+            pltpu.VMEM((nz, rows, width), BF16),
+            pltpu.VMEM((nz, rows, width), BF16),
+            pltpu.VMEM((rows, width), F32),
+            *held[7:],
+            dma((len(streamed),)),
+            dma((3,)),
+            dma((3,)),
+            dma((2,)),
+            dma((2,)),
+            dma((2,)),
+            dma((2,)),
+            dma((nz,)),
+            dma((nz,)),
+            dma((nz,)),
+            dma((nz,)),
+            dma((nz, peers)),
+            dma((nz, peers)),
+            dma((nz, peers)),
+            dma((nz, peers)),
+            dma((nz,)),
+            dma((nz,)),
+        ],
+        compiler_params=pltpu.CompilerParams(
+            collective_id=0, has_side_effects=True, vmem_limit_bytes=67043328
         ),
-        "sp",
-        1,
-    )
-    source = jnp.concatenate(
-        [
-            prev_input.astype(jnp.float32) * prev_value.astype(jnp.float32),
-            conv_input.astype(jnp.float32) * conv_value.astype(jnp.float32),
-        ],
-        axis=0,
-    )
-    doc_extended = jnp.concatenate([prev_doc.astype(jnp.float32), doc_float], axis=0)
-    mixed_conv = jnp.zeros((seq_rows, half_width), jnp.float32)
-    for tap in range(tap_count):
-        same_doc = (doc_extended[tap : tap + seq_rows] == doc_float).astype(jnp.float32)[:, None]
-        mixed_conv = (
-            mixed_conv
-            + conv_taps[tap].astype(jnp.float32)[None, :] * source[tap : tap + seq_rows] * same_doc
-        )
-    branch = outer_gate.astype(jnp.float32) * mixed_conv
-    square_total = lax.psum(jnp.sum(branch * branch, axis=1, keepdims=True), "tp")
-    inv_rms = lax.rsqrt(square_total / (half_width * lax.axis_size("tp")) + norm_eps)
-    normed = (branch * inv_rms * branch_gain.astype(jnp.float32)[None, :]).astype(jnp.bfloat16)
-    local_rows = residual.shape[0]
-    token_rows = lax.all_to_all(normed, "tp", split_axis=0, concat_axis=1, tiled=True)
-    update = jnp.dot(token_rows, out_weight, preferred_element_type=jnp.float32)
-    middle = (residual.astype(jnp.float32) + update).astype(jnp.bfloat16)
-    mid_float = middle.astype(jnp.float32)
-    mid_rms = lax.rsqrt(jnp.mean(mid_float * mid_float, axis=1, keepdims=True) + norm_eps)
-    ffn_in = (mid_float * mid_rms * ffn_gain.astype(jnp.float32)[None, :]).astype(jnp.bfloat16)
-
-    top_count = route_ids.shape[1]
-    core_devices = lax.axis_size("tp")
-    expert_count = lax.axis_size("sp") * core_devices
-    capacity = local_rows * core_devices * top_count // expert_count
-    slots = -(-capacity // 16) * 16
-    ids = route_ids.T
-    experts = jnp.arange(expert_count, dtype=jnp.int32)
-    named = jnp.sum((ids[:, None, :] == experts[None, :, None]).astype(F32), axis=0)
-    token = jnp.arange(local_rows, dtype=jnp.int32)
-    before = (token[:, None] < token[None, :]).astype(BF16)
-    earlier = jnp.dot(named.astype(BF16), before, preferred_element_type=F32)
-    rank = jnp.sum(
-        jnp.where(ids[:, None, :] == experts[None, :, None], earlier[None, :, :], 0.0), axis=1
-    )
-    places = ids.astype(F32) * slots + rank
-    meta = jnp.concatenate([places, route_weight.T], axis=0)
-    return run_experts(
-        ffn_in,
-        meta,
-        middle,
-        (shared_gate, shared_up, shared_down),
-        (expert_gate, expert_up, expert_down),
-        slots,
-    )
+    )(*streamed, *small)
 
 
 def solution(mesh):

time: 169 us -> 139 us (0.82)
  starting transfers between devices: 9.45 us -> 0 us
  other arithmetic: 10.6 us -> 2.05 us
  blocking collectives: 7.56 us -> 0 us
  matrix products: 3.17 us -> 0 us
  Pallas kernels: 133 us -> 131 us
    ppermute x3 -> x0, starting transfers between devices: 9.45 us -> none  [from_behind(): return lax.ppermute(value, axis, pairs)]
    all_to_all x1 -> x0, blocking collectives: 3.92 us -> none  [shards(): lax.all_to_all(normed, 'tp', split_axis=0, concat_axis=1, tiled=True)]
    psum x1 -> x0, blocking collectives: 3.64 us -> none  [shards(): lax.psum(jnp.sum(branch * branch, axis=1, keepdims=True), 'tp')]
    broadcast_in_dim x0 -> x3, local copies, waits for them, and re-layouts: none -> 3.31 us  [the longest x2 2.56 us: shards(): small = (conv_taps, branch_gain[None, :], ffn_gain[None, :])]
    dot_general x2 -> x0, matrix products: 3.17 us -> none  [the longest x1 3.03 us: shards(): update = jnp.dot(token_rows, out_weight, preferred_element_type=jnp.float32)]
    reduce_sum x3 -> x0, other arithmetic: 2.74 us -> none  [the longest x1 1.33 us: shards(): jnp.sum(branch * branch, axis=1, keepdims=True)]
    pallas_call x1, Pallas kernels: 133 us -> 131 us  [shards(): pl.pallas_call(functools.partial(experts_kernel, nz, plane, cores, slots,...]
    mul x3 -> x0, other arithmetic: 1.91 us -> none  [the longest x1 1.1 us: shards(): conv_input.astype(jnp.float32) * conv_value.astype(jnp.float32)]
  transfers between devices with their start and end apart: 3 -> 0, of which waited for: 0 -> 0; matrix products, arithmetic and copies ran while one was open for 5% -> 0% of each run, Pallas kernels for 0% -> 0%
where the time goes in v2:
time: 139 us
  Pallas kernels  131 us (94%)
  local copies, waits for them, and re-layouts  5.92 us (4%)
  other arithmetic  2.05 us (1%)
    pallas_call x1, Pallas kernels, shards(): pl.pallas_call(functools.partial(experts_kernel, nz, plane, cores, slots,...  131 us

profile of v2, /device:TPU:25, one launch (start us, length us, event | category | flops | bytes accessed | tf_op | source)
XLA Modules:
  0.0 138.7 jit_solution(12452931314566796854)
XLA Ops:
  0.0 0.7 convert_element_type.8
  0.7 1.3 broadcast_in_dim.13.branch_gain_ref
  2.0 0.7 convert_element_type.9
  2.6 0.7 pad_maximum_fusion
  3.3 1.3 broadcast_in_dim.14.ffn_gain_ref
  4.6 0.1 copy.20
  4.7 0.6 pad.4.route_hbm
  5.3 0.8 broadcast_in_dim.12.doc_hbm
  6.1 130.7 %shard_map.163 = bf16[128,2048]{1,0:T(8,128)(2,1)} custom-call(bf16[256,512]{1,0:T(8,128)(2,1)} %in_hbm.1, bf16[256,512]{1,0:T(8,128)(2,1)} %val_hbm.1, f32[256,128]{1,0:T(8,128)} %broadcast_in_dim.12.doc_hbm, f32[128,128]{1,0:T(8,128)} %pad.4.route_hbm, bf16[256,512]{1,0:T(8,128)(2,1)} %outer_hbm.1, bf16[1024,2048]{1,0:T(8,128)(2,1)} %ow_hbm.1, ...), custom_call_target="tpu_custom_call" | custom-call | tf_op jit(solution)/shard_map/pallas_call | solution.py:480
  136.8 1.9 %copy.22 = bf16[128,2048]{1,0:T(8,128)(2,1)} copy(bf16[128,2048]{1,0:T(8,128)(2,1)} %shard_map.163) | data formatting | bytes 1048576

commit v3 on v2

--- a/solution.py
+++ b/solution.py
@@ -33,7 +33,8 @@
     in_hbm,
     val_hbm,
     doc_hbm,
-    route_hbm,
+    ids_hbm,
+    weights_hbm,
     outer_hbm,
     ow_hbm,
     residual_hbm,
@@ -50,7 +51,8 @@
     conv_in,
     conv_val,
     docs,
-    route,
+    ids,
+    weights,
     outer,
     ow,
     residual,
@@ -115,7 +117,8 @@
                 (in_hbm, conv_in),
                 (val_hbm, conv_val),
                 (doc_hbm, docs),
-                (route_hbm, route),
+                (ids_hbm, ids),
+                (weights_hbm, weights),
                 (outer_hbm, outer),
                 (ow_hbm, ow),
                 (residual_hbm, residual),
@@ -151,7 +154,7 @@
     behind = ((me_sp + seq_devices - 1) % seq_devices, me_tp)
     pl.semaphore_signal(barrier, inc=1, device_id=ahead, device_id_type=MESH)
     pl.semaphore_signal(barrier, inc=1, device_id=behind, device_id_type=MESH)
-    for load in loads[:4]:
+    for load in loads[:5]:
         load.wait()
     pl.semaphore_wait(barrier, nz - 1 + peers - 1 + 2)
 
@@ -174,7 +177,7 @@
         copy.start()
 
     rows_here = residual.shape[0]
-    named_by = route[...].T
+    named_by = ids[...].astype(F32)
     experts = lax.broadcasted_iota(jnp.int32, (expert_count, rows_here), 0).astype(F32)
     matches = [experts == named_by[k : k + 1, :] for k in range(tops)]
     named = jnp.zeros((expert_count, rows_here), F32)
@@ -186,10 +189,10 @@
     for k, match in enumerate(matches):
         rank = jnp.sum(jnp.where(match, earlier, 0.0), axis=0, keepdims=True)
         gmeta[me_z, k : k + 1, :] = named_by[k : k + 1, :] * slots + rank
-        gmeta[me_z, tops + k : tops + k + 1, :] = named_by[tops + k : tops + k + 1, :]
+        gmeta[me_z, tops + k : tops + k + 1, :] = weights[k : k + 1, :]
 
     source[lead:, :] = conv_in[...].astype(F32) * conv_val[...].astype(F32)
-    for load in loads[4:7]:
+    for load in loads[5:8]:
         load.wait()
     for copy in halo_copies:
         copy.wait_recv()
@@ -215,7 +218,7 @@
             mixed = mixed + jnp.where(same[tap], weight * lagged, 0.0)
         branch = outer[:, part].astype(F32) * mixed
         total_square = total_square + jnp.sum(branch * branch, axis=1, keepdims=True)
-        scaled[:, part] = (branch * branch_gain_ref[:, part].astype(F32)).astype(BF16)
+        scaled[:, part] = (branch * branch_gain_ref[part].astype(F32)[None, :]).astype(BF16)
     squares[...] = jnp.broadcast_to(total_square, squares.shape)
 
     other_tp = 1 - me_tp
@@ -240,7 +243,7 @@
     middle = (residual[...].astype(F32) + update).astype(BF16).astype(F32)
     mid_rms = lax.rsqrt(jnp.mean(middle * middle, axis=1, keepdims=True) + norm_eps)
     acc[...] = middle
-    gath[me_z] = (middle * mid_rms * ffn_gain_ref[...].astype(F32)).astype(BF16)
+    gath[me_z] = (middle * mid_rms * ffn_gain_ref[...].astype(F32)[None, :]).astype(BF16)
 
     def block_of(r):
         fewer = jnp.minimum(me_z, nz - 1 - me_z)
@@ -373,13 +376,13 @@
 
         @pl.when(i == 0)
         def _():
-            for load in loads[7:10]:
+            for load in loads[8:11]:
                 load.wait()
             rows = gath[me_z]
             gate = dot(rows, sg[...])
             hidden = (gate / (1.0 + jnp.exp(-gate)) * dot(rows, su[...])).astype(BF16)
             acc[...] += dot(hidden, sd[...])
-            for load in loads[10:]:
+            for load in loads[11:]:
                 load.wait()
 
         @pl.when((i >= 1) & (i <= nz))
@@ -455,13 +458,12 @@
     slots = -(-capacity // 16) * 16
     lanes = 128
     docs = jnp.broadcast_to(doc_ids.astype(F32)[:, None], (seq_rows, lanes))
-    route = jnp.concatenate([route_ids.astype(F32), route_weight], axis=1)
-    route = jnp.pad(route, ((0, 0), (0, lanes - 2 * tops)))
     streamed = (
         conv_input,
         conv_value,
         docs,
-        route,
+        route_ids.T,
+        route_weight.T,
         outer_gate,
         out_weight,
         residual,
@@ -473,7 +475,7 @@
         expert_down,
     )
     held = [pltpu.VMEM(a.shape, a.dtype) for a in streamed]
-    small = (conv_taps, branch_gain[None, :], ffn_gain[None, :])
+    small = (conv_taps, branch_gain, ffn_gain)
     dma = pltpu.SemaphoreType.DMA
     tile = (nz, peers, slots, width)
     lead, packed = 8, 16
@@ -484,7 +486,7 @@
         + [pl.BlockSpec(memory_space=pltpu.VMEM)] * len(small),
         out_specs=pl.BlockSpec(memory_space=pltpu.VMEM),
         scratch_shapes=[
-            *held[:7],
+            *held[:8],
             pltpu.VMEM((lead + seq_rows, half_width), F32),
             pltpu.VMEM((packed, half_width), BF16),
             pltpu.VMEM((packed, half_width), BF16),
@@ -502,7 +504,7 @@
             pltpu.VMEM((nz, rows, width), BF16),
             pltpu.VMEM((nz, rows, width), BF16),
             pltpu.VMEM((rows, width), F32),
-            *held[7:],
+            *held[8:],
             dma((len(streamed),)),
             dma((3,)),
             dma((3,)),

time: 139 us -> 134 us (0.964)
  local copies, waits for them, and re-layouts: 5.92 us -> 2.64 us
    broadcast_in_dim x2 -> x0, local copies, waits for them, and re-layouts: 2.56 us -> none  [shards(): small = (conv_taps, branch_gain[None, :], ffn_gain[None, :])]
where the time goes in v3:
time: 134 us
  Pallas kernels  131 us (98%)
  local copies, waits for them, and re-layouts  2.64 us (2%)
    pallas_call x1, Pallas kernels, shards(): pl.pallas_call(functools.partial(experts_kernel, nz, plane, cores, slots,...  131 us

profile of v3, /device:TPU:25, one launch (start us, length us, event | category | flops | bytes accessed | tf_op | source)
XLA Modules:
  0.0 134.2 jit_solution(3205022798507024028)
XLA Ops:
  0.0 0.7 convert_element_type.3
  0.7 0.8 broadcast_in_dim.2.doc_hbm
  1.4 130.9 %shard_map.163 = bf16[128,2048]{1,0:T(8,128)(2,1)} custom-call(bf16[256,512]{1,0:T(8,128)(2,1)} %in_hbm.1, bf16[256,512]{1,0:T(8,128)(2,1)} %val_hbm.1, f32[256,128]{1,0:T(8,128)} %broadcast_in_dim.2.doc_hbm, s32[4,128]{1,0:T(4,128)} %bitcast.2, f32[4,128]{1,0:T(4,128)} %bitcast.3, bf16[256,512]{1,0:T(8,128)(2,1)} %outer_hbm.1, bf16[1024,2048]{1,0:T(8,128)(2,1)} %ow_hbm.1, ...), custom_call_target="tpu_custom_call" | custom-call | tf_op jit(solution)/shard_map/pallas_call | solution.py:482
  132.3 1.9 %copy.19 = bf16[128,2048]{1,0:T(8,128)(2,1)} copy(bf16[128,2048]{1,0:T(8,128)(2,1)} %shard_map.163) | data formatting | bytes 1048576
